TPU v7x, 32 devices: a whole 2x2x4 slice. The times are simulated.
32 devices in a mesh: grp: 2 (over y), fs: 4 (over z), tp: 4 (over x, core).
Axes of the slice: x: 2, y: 2, z: 4, core: 2. Of those that a mesh axis runs over, the one named last changes fastest.
Arguments:
- tokens: bfloat16 [8192, 2048], P(('grp', 'fs')), parts along dimension 0, may hold values from -6 to 6
- mixer_gain: float32 [2048], replicated, may hold values from 0.1 to 1.9
- outer_weight: float32 [2048, 2048], P('fs', 'tp'), may hold values from -0.125 to 0.125
- inner_weight: float32 [2048, 2048], P('fs', 'tp'), may hold values from -0.125 to 0.125
- value_weight: float32 [2048, 2048], P('fs', 'tp'), may hold values from -0.125 to 0.125
- filter_taps: float32 [3, 2048], P(None, 'tp'), may hold values from -3.5 to 3.5
- mixer_weight: float32 [2048, 2048], P('tp', 'fs'), may hold values from -0.125 to 0.125
- outer_scale: float32 [4, 512], P('tp', 'fs'), may hold values from 0.5 to 2
- inner_scale: float32 [4, 512], P('tp', 'fs'), may hold values from 0.5 to 2
- value_scale: float32 [4, 512], P('tp', 'fs'), may hold values from 0.5 to 2
- mixer_scale: float32 [1, 2048], P(None, 'fs'), may hold values from 0.5 to 2
Outputs:
- layer_out: bfloat16 [8192, 2048], P(('grp', 'fs', 'tp')), parts along dimension 0
There are 2 independent parts, one for each index of `grp`. A program takes and returns all parts, laid end to end along the dimension named above; an argument that names none is the same for every part. Nothing has to cross between parts.
All inputs are finite; a program needn't handle non-finite values.
Results may differ from a plain program's by a relative error of at most 0.014.
Values may be sent and summed in bfloat16 or wider, within the bound.
A program may use at most 64 MiB of HBM per device.

v0:
```python
import jax
import jax.numpy as jnp
from jax import lax
from jax.sharding import PartitionSpec as P

EPS = 1e-06


def normed(rows, gain):
    values = rows.astype(jnp.float32)
    inverse = lax.rsqrt(jnp.mean(values * values, axis=-1, keepdims=True) + EPS)
    return (values * inverse * gain).astype(jnp.bfloat16)


def rounded(values):
    return lax.optimization_barrier(values.astype(jnp.bfloat16)).astype(jnp.float32)


def add_rows(left, piece):
    return jnp.dot(left, piece, preferred_element_type=jnp.float32)


def per_device(
    tokens,
    mixer_gain,
    outer_weight,
    inner_weight,
    value_weight,
    filter_taps,
    mixer_weight,
    outer_scale,
    inner_scale,
    value_scale,
    mixer_scale,
):
    gathered = (
        lax.all_gather(outer_scale, "fs", axis=1, tiled=True),
        lax.all_gather(inner_scale, "fs", axis=1, tiled=True),
        lax.all_gather(value_scale, "fs", axis=1, tiled=True),
        lax.all_gather(mixer_scale, "fs", axis=1, tiled=True),
    )
    outer_col, inner_col, value_col, mixer_col = [piece.reshape(-1) for piece in gathered]
    seq_rows = tokens.shape[0]
    normal_rows = normed(tokens, mixer_gain)

    def fold_one(piece):
        return add_rows(normal_rows, piece)

    outer_sum = fold_one(
        lax.all_gather(outer_weight.astype(jnp.bfloat16), "fs", axis=0, tiled=True)
    )
    inner_sum = fold_one(
        lax.all_gather(inner_weight.astype(jnp.bfloat16), "fs", axis=0, tiled=True)
    )
    value_sum = fold_one(
        lax.all_gather(value_weight.astype(jnp.bfloat16), "fs", axis=0, tiled=True)
    )
    outer = rounded(outer_sum * outer_col)
    inner = rounded(inner_sum * inner_col)
    value = rounded(value_sum * value_col)
    padded = jnp.pad(inner * value, ((2, 0), (0, 0)))
    filtered = (
        filter_taps[0] * padded[0:seq_rows]
        + filter_taps[1] * padded[1 : seq_rows + 1]
        + filter_taps[2] * padded[2:]
    )
    gated = (outer * filtered).astype(jnp.bfloat16)
    mixer_full = lax.all_gather(mixer_weight.astype(jnp.bfloat16), "fs", axis=1, tiled=True)
    return lax.psum_scatter(
        (jnp.dot(gated, mixer_full, preferred_element_type=jnp.float32) * mixer_col).astype(
            jnp.bfloat16
        ),
        "tp",
        scatter_dimension=0,
        tiled=True,
    )


def solution(mesh):
    in_specs = (
        P(("grp", "fs"), None),
        P(),
        P("fs", "tp"),
        P("fs", "tp"),
        P("fs", "tp"),
        P(None, "tp"),
        P("tp", "fs"),
        P("tp", "fs"),
        P("tp", "fs"),
        P("tp", "fs"),
        P(None, "fs"),
    )
    out_specs = P(("grp", "fs", "tp"), None)
    return jax.shard_map(
        per_device, mesh=mesh, in_specs=in_specs, out_specs=out_specs, check_vma=False
    )
```

profile of v0, /device:TPU:1, one launch (start us, length us, event | category | flops | bytes accessed | tf_op | source)
XLA Modules:
  0.0 251.5 jit_solution(7031129598482165264)
XLA Ops:
  6.5 2.2 convert_element_type.46
  8.8 0.0 all-gather.5.cloned.1.call-update
  8.8 0.0 all-gather.7.cloned.1.call-start
  8.9 0.9 convert_element_type.49
  9.8 0.0 all-gather.9.cloned.1.call-start
  9.9 0.9 convert_element_type.52
  10.8 0.0 all-gather.11.cloned.1.call-start
  10.8 0.9 convert_element_type.56
  11.8 0.0 reduce-scatter.2.cloned.1.call-start
  11.8 10.0 %all_gather.25 = f32[1,512]{1,0:T(1,128)S(1)} all-gather(f32[1,128]{1,0:T(1,128)S(1)} %copy-done.5), channel_id=1, replica_groups=mesh['grp'=2,'fs'=4,'tp'=4] {'fs'}, dimensions={1}, use_global_device_ids=true | all-gather | bytes 2560 | tf_op jit(solution)/shard_map/all_gather | solution.py:37
  21.8 6.3 %all_gather.27 = f32[1,512]{1,0:T(1,128)S(1)} all-gather(f32[1,128]{1,0:T(1,128)S(1)} %copy-done.6), channel_id=1, replica_groups=mesh['grp'=2,'fs'=4,'tp'=4] {'fs'}, dimensions={1}, use_global_device_ids=true | all-gather | bytes 2560 | tf_op jit(solution)/shard_map/all_gather | solution.py:38
  28.1 8.1 %all_gather.29 = f32[1,512]{1,0:T(1,128)S(1)} all-gather(f32[1,128]{1,0:T(1,128)S(1)} %copy-done.7), channel_id=1, replica_groups=mesh['grp'=2,'fs'=4,'tp'=4] {'fs'}, dimensions={1}, use_global_device_ids=true | all-gather | bytes 2560 | tf_op jit(solution)/shard_map/all_gather | solution.py:39
  36.2 10.3 %all_gather.31 = f32[1,2048]{1,0:T(1,128)S(1)} all-gather(f32[1,512]{1,0:T(1,128)S(1)} %copy-done.4), channel_id=1, replica_groups=mesh['grp'=2,'fs'=4,'tp'=4] {'fs'}, dimensions={1}, use_global_device_ids=true | all-gather | bytes 10240 | tf_op jit(solution)/shard_map/all_gather | solution.py:40
  46.5 3.1 %fusion = f32[1024]{0:T(1024)S(1)} fusion(bf16[1024,2048]{1,0:T(8,128)(2,1)} %param.11), kind=kLoop, calls=%fused_computation.2 | loop fusion | flops 6290432 | bytes 4198400 | tf_op jit(solution)/shard_map/reduce_sum | solution.py:11
  49.6 7.1 %all-gather.5.cloned.1.call-done = bf16[2048,512]{1,0:T(8,128)(2,1)} async-done(((bf16[512,512]{1,0:T(8,128)(2,1)}), bf16[2048,512]{1,0:T(8,128)(2,1)}) %all-gather.5.cloned.1.call-update) | async-done | bytes 2097168 | tf_op jit(solution)/shard_map/all_gather | solution.py:50
  56.7 6.2 %multiply_convert_fusion.4 = bf16[1024,512]{1,0:T(8,128)(2,1)} fusion(bf16[2048,512]{1,0:T(8,128)(2,1)} %all-gather.5.cloned.1.call-done, f32[512]{0:T(512)S(1)} %bitcast.14, bf16[1024,2048]{1,0:T(8,128)(2,1)} %param.11, f32[2048]{0:T(1024)S(1)} %copy-done.8, f32[1024]{0:T(1024)S(1)} %add_rsqrt_fusion), kind=kOutput, calls=%fused_computation.10 | convolution fusion | flops 2156920832 | bytes 7354368 | tf_op jit(solution)/shard_map/dot_general | solution.py:20
  62.9 39.8 %all-gather.7.cloned.1.call-done = bf16[2048,512]{1,0:T(8,128)(2,1)} async-done(((bf16[512,512]{1,0:T(8,128)(2,1)}), bf16[2048,512]{1,0:T(8,128)(2,1)}) %all-gather.7.cloned.1.call-update) | async-done | bytes 2097168 | tf_op jit(solution)/shard_map/all_gather | solution.py:53
  102.8 5.2 %multiply_convert_fusion.3 = bf16[1024,512]{1,0:T(8,128)(2,1)S(1)} fusion(bf16[2048,512]{1,0:T(8,128)(2,1)} %all-gather.7.cloned.1.call-done, f32[512]{0:T(512)S(1)} %bitcast.13, bf16[1024,2048]{1,0:T(8,128)(2,1)} %param.11, f32[2048]{0:T(1024)S(1)} %copy-done.8, f32[1024]{0:T(1024)S(1)} %add_rsqrt_fusion), kind=kOutput, calls=%fused_computation.9 | convolution fusion | flops 2156920832 | bytes 7354368 | tf_op jit(solution)/shard_map/dot_general | solution.py:20
  108.0 40.8 %all-gather.9.cloned.1.call-done = bf16[2048,512]{1,0:T(8,128)(2,1)} async-done(((bf16[512,512]{1,0:T(8,128)(2,1)}), bf16[2048,512]{1,0:T(8,128)(2,1)}) %all-gather.9.cloned.1.call-update) | async-done | bytes 2097168 | tf_op jit(solution)/shard_map/all_gather | solution.py:56
  148.8 5.2 %multiply_convert_fusion.2 = bf16[1024,512]{1,0:T(8,128)(2,1)S(1)} fusion(bf16[2048,512]{1,0:T(8,128)(2,1)} %all-gather.9.cloned.1.call-done, f32[512]{0:T(512)S(1)} %bitcast.12, bf16[1024,2048]{1,0:T(8,128)(2,1)} %param.11, f32[2048]{0:T(1024)S(1)} %copy-done.8, f32[1024]{0:T(1024)S(1)} %add_rsqrt_fusion), kind=kOutput, calls=%fused_computation.8 | convolution fusion | flops 2156920832 | bytes 7354368 | tf_op jit(solution)/shard_map/dot_general | solution.py:20
  154.1 0.3 convert_multiply_fusion.2
  154.4 40.4 %all-gather.11.cloned.1.call-done = bf16[512,2048]{1,0:T(8,128)(2,1)} async-done(((bf16[512,512]{1,0:T(8,128)(2,1)}), bf16[512,2048]{1,0:T(8,128)(2,1)}) %all-gather.11.cloned.1.call-update) | async-done | bytes 2097168 | tf_op jit(solution)/shard_map/all_gather | solution.py:68
  194.8 6.6 %multiply_convert_fusion = bf16[1024,2048]{1,0:T(8,128)(2,1)} fusion(bf16[512,2048]{1,0:T(8,128)(2,1)} %all-gather.11.cloned.1.call-done, f32[2048]{0:T(1024)S(1)} %bitcast.11, f32[1024,512]{1,0:T(8,128)S(1)} %convert_multiply_fusion.2, bf16[1024,512]{1,0:T(8,128)(2,1)} %multiply_convert_fusion.4, f32[512]{0:T(512)S(1)} %bitcast.16, f32[512]{0:T(512)S(1)} %bitcast.17, ...), kind=kOutput, calls=%fused_computation.5 | convolution fusion | flops 2155872256 | bytes 9451520 | tf_op jit(solution)/shard_map/dot_general | solution.py:70
  201.4 43.6 %reduce-scatter.2.cloned.1.call-done = bf16[256,2048]{1,0:T(8,128)(2,1)} async-done(((bf16[1024,2048]{1,0:T(8,128)(2,1)}), bf16[256,2048]{1,0:T(8,128)(2,1)}) %reduce-scatter.2.cloned.1.call-update) | async-done | bytes 1048592 | tf_op jit(solution)/shard_map/reduce_scatter | solution.py:69
  (25 shorter events, 0.1 us)
Async XLA Ops:
  6.5 2.3 copy-start
  6.5 3.3 %copy-start.1 = (f32[512,512]{1,0:T(8,128)S(1)}, f32[512,512]{1,0:T(8,128)}, u32[]{:S(2)}) copy-start(f32[512,512]{1,0:T(8,128)} %param.15) | copy-start | bytes 3145732
  6.5 50.2 %all-gather.5.cloned.1.call-start = ((), (), s32[]{:S(2)}) async-start(), calls=%async_computation.1 | async-start | bytes 2621440 | tf_op jit(solution)/shard_map/all_gather | solution.py:50
  8.8 2.0 copy-start.2
  8.8 94.0 %all-gather.7.cloned.1.call-start = ((), (), s32[]{:S(2)}) async-start(), calls=%async_computation.2 | async-start | bytes 2621440 | tf_op jit(solution)/shard_map/all_gather | solution.py:53
  9.8 2.1 copy-start.5
  9.8 12.0 %copy-start.6 = (f32[1,128]{1,0:T(1,128)S(1)}, f32[1,128]{1,0:T(1,128)}, u32[]{:S(2)}) copy-start(f32[1,128]{1,0:T(1,128)} %param.19) | copy-start | bytes 1540
  9.8 18.3 %copy-start.7 = (f32[1,128]{1,0:T(1,128)S(1)}, f32[1,128]{1,0:T(1,128)}, u32[]{:S(2)}) copy-start(f32[1,128]{1,0:T(1,128)} %param.20) | copy-start | bytes 1540
  9.8 26.4 %copy-start.4 = (f32[1,512]{1,0:T(1,128)S(1)}, f32[1,512]{1,0:T(1,128)}, u32[]{:S(2)}) copy-start(f32[1,512]{1,0:T(1,128)} %param.21) | copy-start | bytes 6148
  9.8 139.0 %all-gather.9.cloned.1.call-start = ((), (), s32[]{:S(2)}) async-start(), calls=%async_computation.3 | async-start | bytes 2621440 | tf_op jit(solution)/shard_map/all_gather | solution.py:56
  10.8 184.0 %all-gather.11.cloned.1.call-start = ((), (), s32[]{:S(2)}) async-start(), calls=%async_computation.4 | async-start | bytes 2621440 | tf_op jit(solution)/shard_map/all_gather | solution.py:68
  11.8 233.2 %reduce-scatter.2.cloned.1.call-start = ((), (), s32[]{:S(2)}) async-start(), calls=%async_computation.5 | async-start | bytes 5242880 | tf_op jit(solution)/shard_map/reduce_scatter | solution.py:69
  46.5 3.1 %copy-start.3 = (f32[3,512]{1,0:T(4,128)S(1)}, f32[3,512]{1,0:T(4,128)}, u32[]{:S(2)}) copy-start(f32[3,512]{1,0:T(4,128)} %param.16) | copy-start | bytes 18436
  46.5 10.2 %copy-start.8 = (f32[2048]{0:T(1024)S(1)}, f32[2048]{0:T(1024)}, u32[]{:S(2)}) copy-start(f32[2048]{0:T(1024)} %param.12) | copy-start | bytes 24580
Sparse Core Ops, SparseCore 0:
  8.9 47.7 all-gather.4
  58.3 44.4 all-gather.6
  104.3 44.4 all-gather.8
  150.3 44.4 all-gather.10
  201.5 43.3 reduce-scatter.1
where the time goes:
time: 252 us; the launch traced here: 251 us
  waiting for transfers between devices  172 us (68%)
  blocking collectives  34.6 us (14%)
  matrix products  23.3 us (9%)
  between operations  13.3 us (5%)
  other arithmetic  8.31 us (3%)
    reduce_scatter x1, waiting for transfers between devices, per_device(): lax.psum_scatter((jnp.dot(gated, mixer_full, preferred_element_type=jnp.f...  43.6 us
    all_gather x1, waiting for transfers between devices, per_device(): lax.all_gather(value_weight.astype(jnp.bfloat16), 'fs', axis=0, tiled=True)  40.8 us
    all_gather x1, waiting for transfers between devices, per_device(): lax.all_gather(mixer_weight.astype(jnp.bfloat16), 'fs', axis=1, tiled=True)  40.4 us
    all_gather x1, waiting for transfers between devices, per_device(): lax.all_gather(inner_weight.astype(jnp.bfloat16), 'fs', axis=0, tiled=True)  39.8 us
    dot_general x3, matrix products, add_rows(): return jnp.dot(left, piece, preferred_element_type=jnp.float32)  16.7 us
    all_gather x1, blocking collectives, per_device(): lax.all_gather(mixer_scale, 'fs', axis=1, tiled=True)  10.3 us
    all_gather x1, blocking collectives, per_device(): lax.all_gather(outer_scale, 'fs', axis=1, tiled=True)  9.96 us
    all_gather x1, blocking collectives, per_device(): lax.all_gather(value_scale, 'fs', axis=1, tiled=True)  8.08 us
  transfers between devices with their start and end apart: 5, of which 5 were waited for; matrix products, arithmetic and copies ran while one was open for 9% of the time, Pallas kernels for 0%

commit v1 on v0

--- a/solution.py
+++ b/solution.py
@@ -1,6 +1,10 @@
+import functools
+
 import jax
 import jax.numpy as jnp
 from jax import lax
+from jax.experimental import pallas as pl
+from jax.experimental.pallas import tpu as pltpu
 from jax.sharding import PartitionSpec as P
 
 EPS = 1e-06
@@ -76,6 +80,457 @@
     )
 
 
+MESH = pl.DeviceIdType.MESH
+MATRICES = 4
+
+
+def mixer_kernel(
+    n,
+    tokens_hbm,
+    gain_ref,
+    w0_hbm,
+    w1_hbm,
+    w2_hbm,
+    taps_ref,
+    w3_hbm,
+    s0_ref,
+    s1_ref,
+    s2_ref,
+    s3_ref,
+    out_ref,
+    toks,
+    rows,
+    stage,
+    held,
+    scales,
+    outer_buf,
+    inner_buf,
+    product,
+    gated,
+    own_part,
+    core_out,
+    core_in,
+    chip_out,
+    chip_in,
+    load_sem,
+    zl_sem,
+    zr_sem,
+    zin_sem,
+    yout_sem,
+    yin_sem,
+    sout_sem,
+    sin_sem,
+    cout_sem,
+    cin_sem,
+    xout_sem,
+    xin_sem,
+):
+    z = lax.axis_index("fs")
+    y = lax.axis_index("grp")
+    t = lax.axis_index("tp")
+    ntp = 4
+    block, width = stage.shape[1], stage.shape[2]
+    half = block // 2
+    seq = rows.shape[0]
+    tile = seq // ntp
+    partner = t + 1 - 2 * lax.rem(t, 2)
+    across = lax.rem(t + 2, ntp)
+    x, core = t // 2, lax.rem(t, 2)
+    weights = (w0_hbm, w1_hbm, w2_hbm, w3_hbm)
+
+    loads = [
+        pltpu.make_async_copy(weights[m], stage.at[m], load_sem.at[m]) for m in range(MATRICES)
+    ]
+    token_load = pltpu.make_async_copy(tokens_hbm, toks, load_sem.at[MATRICES])
+    for load in loads:
+        load.start()
+    token_load.start()
+
+    barrier = pltpu.get_barrier_semaphore()
+    for d in range(1, n):
+        pl.semaphore_signal(
+            barrier, inc=1, device_id={"fs": lax.rem(z + d, n)}, device_id_type=MESH
+        )
+    for d in range(1, ntp):
+        pl.semaphore_signal(
+            barrier, inc=1, device_id={"tp": lax.rem(t + d, ntp)}, device_id_type=MESH
+        )
+    pl.semaphore_signal(barrier, inc=1, device_id={"grp": 1 - y}, device_id_type=MESH)
+
+    q = s0_ref.shape[1]
+    scales[z, :, 0:q] = s0_ref[...]
+    scales[z, :, q : 2 * q] = s1_ref[...]
+    scales[z, :, 2 * q : 3 * q] = s2_ref[...]
+    scales[z, :, 3 * q :] = s3_ref[...]
+
+    def cast(m):
+        loads[m].wait()
+        held[m, pl.ds(pl.multiple_of(z * block, block), block), :] = stage[m].astype(jnp.bfloat16)
+
+    def part_of(m, b):
+        return held.at[m, pl.ds(pl.multiple_of(b * block + y * half, half), half), :]
+
+    def other_of(m, b):
+        return held.at[m, pl.ds(pl.multiple_of(b * block + (1 - y) * half, half), half), :]
+
+    def to_left(m, b):
+        return pltpu.make_async_remote_copy(
+            src_ref=part_of(m, b),
+            dst_ref=part_of(m, b),
+            send_sem=zl_sem.at[m, b],
+            recv_sem=zin_sem.at[m, b],
+            device_id={"fs": z - 1},
+            device_id_type=MESH,
+        )
+
+    def to_right(m, b):
+        return pltpu.make_async_remote_copy(
+            src_ref=part_of(m, b),
+            dst_ref=part_of(m, b),
+            send_sem=zr_sem.at[m, b],
+            recv_sem=zin_sem.at[m, b],
+            device_id={"fs": z + 1},
+            device_id_type=MESH,
+        )
+
+    def to_twin(m, b):
+        return pltpu.make_async_remote_copy(
+            src_ref=part_of(m, b),
+            dst_ref=part_of(m, b),
+            send_sem=yout_sem.at[m, b],
+            recv_sem=yin_sem.at[m, b],
+            device_id={"grp": 1 - y},
+            device_id_type=MESH,
+        )
+
+    def from_twin(m, b):
+        return pltpu.make_async_remote_copy(
+            src_ref=other_of(m, b),
+            dst_ref=other_of(m, b),
+            send_sem=yout_sem.at[m, b],
+            recv_sem=yin_sem.at[m, b],
+            device_id={"grp": 1 - y},
+            device_id_type=MESH,
+        )
+
+    def scale_copy(d):
+        return pltpu.make_async_remote_copy(
+            src_ref=scales.at[z],
+            dst_ref=scales.at[z],
+            send_sem=sout_sem.at[d],
+            recv_sem=sin_sem.at[z],
+            device_id={"fs": lax.rem(z + d, n)},
+            device_id_type=MESH,
+        )
+
+    def scale_arrival(d):
+        source = lax.rem(z + d, n)
+        return pltpu.make_async_remote_copy(
+            src_ref=scales.at[source],
+            dst_ref=scales.at[source],
+            send_sem=sout_sem.at[d],
+            recv_sem=sin_sem.at[source],
+            device_id={"fs": source},
+            device_id_type=MESH,
+        )
+
+    def send_own(m):
+        @pl.when(z >= 1)
+        def _():
+            to_left(m, z).start()
+
+        @pl.when(z <= n - 2)
+        def _():
+            to_right(m, z).start()
+
+    def relay(m, s):
+        from_right, from_left = z + 1 + s, z - 1 - s
+
+        @pl.when(from_right <= n - 1)
+        def _():
+            to_left(m, from_right).wait_recv()
+
+            @pl.when(z >= 1)
+            def _():
+                to_left(m, from_right).start()
+
+            to_twin(m, from_right).start()
+
+        @pl.when(from_left >= 0)
+        def _():
+            to_right(m, from_left).wait_recv()
+
+            @pl.when(z <= n - 2)
+            def _():
+                to_right(m, from_left).start()
+
+            to_twin(m, from_left).start()
+
+    def twin_arrival(m, s):
+        @pl.when(z + 1 + s <= n - 1)
+        def _():
+            from_twin(m, z + 1 + s).wait_recv()
+
+        @pl.when(z - 1 - s >= 0)
+        def _():
+            from_twin(m, z - 1 - s).wait_recv()
+
+    def column(k):
+        return jnp.concatenate([scales[b, :, k * q : (k + 1) * q] for b in range(n)], axis=1)
+
+    def project(m, first, count):
+        return jnp.dot(
+            rows[first : first + count, :], held[m], preferred_element_type=jnp.float32
+        ) * column(m)
+
+    def project_tiles(m, target, start, stop):
+        for i in range(start, stop):
+            first = i * tile
+            target[first : first + tile, :] = project(m, first, tile).astype(jnp.bfloat16)
+
+    cast(0)
+    cast(1)
+    pl.semaphore_wait(barrier, n - 1 + ntp - 1 + 1)
+    send_own(0)
+    for d in range(1, n):
+        scale_copy(d).start()
+    cast(2)
+    cast(3)
+
+    token_load.wait()
+    strip = seq // 8
+
+    @pl.loop(0, 8)
+    def _(i):
+        at = pl.ds(pl.multiple_of(i * strip, strip), strip)
+        rows[at, :] = normed(toks[at, :], gain_ref[...])
+
+    for d in range(1, n):
+        scale_arrival(d).wait_recv()
+
+    product[0:8, :] = jnp.zeros((8, width), jnp.float32)
+
+    def gate_tile(i):
+        first = i * tile
+        value = project(2, first, tile).astype(jnp.bfloat16).astype(jnp.float32)
+        product[8 + first : 8 + first + tile, :] = (
+            inner_buf[first : first + tile, :].astype(jnp.float32) * value
+        )
+        filtered = (
+            taps_ref[0:1, :] * product[6 + first : 6 + first + tile, :]
+            + taps_ref[1:2, :] * product[7 + first : 7 + first + tile, :]
+            + taps_ref[2:3, :] * product[8 + first : 8 + first + tile, :]
+        )
+        outer = outer_buf[first : first + tile, :].astype(jnp.float32)
+        gated[first : first + tile, :] = (outer * filtered).astype(jnp.bfloat16)
+
+    def core_copy(b):
+        return pltpu.make_async_remote_copy(
+            src_ref=core_out.at[b],
+            dst_ref=core_in.at[b],
+            send_sem=cout_sem.at[b],
+            recv_sem=cin_sem.at[b],
+            device_id={"tp": partner},
+            device_id_type=MESH,
+        )
+
+    def chip_copy(b):
+        return pltpu.make_async_remote_copy(
+            src_ref=chip_out.at[b],
+            dst_ref=chip_in.at[b],
+            send_sem=xout_sem.at[b],
+            recv_sem=xin_sem.at[b],
+            device_id={"tp": across},
+            device_id_type=MESH,
+        )
+
+    def mix_rows(b, index):
+        at = pl.ds(pl.multiple_of(index * tile, tile), tile)
+        weight = held[3, pl.ds(pl.multiple_of(b * block, block), block), :]
+        return (
+            jnp.dot(gated[at, :], weight, preferred_element_type=jnp.float32)
+            * scales[b, :, 3 * q :]
+        )
+
+    def mix(b):
+        for k in range(2):
+            core_out[b, k] = mix_rows(b, 2 * k + 1 - core).astype(jnp.bfloat16)
+        core_copy(b).start()
+        for k in range(2):
+            own_part[b, k] = mix_rows(b, 2 * k + core)
+        core_copy(b).wait_recv()
+        chip_out[b] = (own_part[b, 1 - x] + core_in[b, 1 - x].astype(jnp.float32)).astype(
+            jnp.bfloat16
+        )
+        chip_copy(b).start()
+
+    def mix_arrived(s):
+        @pl.loop(0, 2)
+        def _(side):
+            b = z + (1 + s) * (1 - 2 * side)
+
+            @pl.when((b >= 0) & (b <= n - 1))
+            def _():
+                from_twin(3, b).wait_recv()
+                mix(b)
+
+    steps = [(m, s) for m in range(MATRICES) for s in range(n - 1)]
+    work = {}
+    for m, target in ((0, outer_buf), (1, inner_buf)):
+        at = (m + 1) * (n - 1)
+        work[at + 1] = [functools.partial(project_tiles, m, target, 0, 2)]
+        work[at + 2] = [functools.partial(project_tiles, m, target, 2, 4)]
+    last = 3 * (n - 1)
+    work[last + 1] = [functools.partial(gate_tile, i) for i in range(2)]
+    work[last + 2] = [functools.partial(gate_tile, i) for i in range(2, 4)]
+    for at, (m, s) in enumerate(steps):
+        relay(m, s)
+        if s == n - 2 and m < MATRICES - 1:
+            send_own(m + 1)
+        if at >= 1 and steps[at - 1][0] < 3:
+            twin_arrival(*steps[at - 1])
+        for task in work.get(at, ()):
+            task()
+    mix(z)
+    for s in range(n - 1):
+        mix_arrived(s)
+
+    @pl.loop(0, n)
+    def _(b):
+        chip_copy(b).wait_recv()
+        out_ref[b] = (
+            own_part[b, x]
+            + core_in[b, x].astype(jnp.float32)
+            + chip_in[b].astype(jnp.float32)
+        ).astype(jnp.bfloat16)
+        core_copy(b).wait_send()
+        chip_copy(b).wait_send()
+
+    for d in range(1, n):
+        scale_copy(d).wait_send()
+    for m in range(MATRICES):
+
+        @pl.loop(0, n)
+        def _(b):
+            @pl.when((b >= z) & (z >= 1))
+            def _():
+                to_left(m, b).wait_send()
+
+            @pl.when((b <= z) & (z <= n - 2))
+            def _():
+                to_right(m, b).wait_send()
+
+            @pl.when(b != z)
+            def _():
+                to_twin(m, b).wait_send()
+
+
+def fused_device(
+    n,
+    tokens,
+    mixer_gain,
+    outer_weight,
+    inner_weight,
+    value_weight,
+    filter_taps,
+    mixer_weight,
+    outer_scale,
+    inner_scale,
+    value_scale,
+    mixer_scale,
+):
+    seq, depth = tokens.shape
+    block, width = outer_weight.shape
+    tile = seq // 4
+    whole = pl.BlockSpec(memory_space=pltpu.VMEM)
+    anywhere = pl.BlockSpec(memory_space=pl.ANY)
+    bf16, f32 = jnp.bfloat16, jnp.float32
+    dma = pltpu.SemaphoreType.DMA
+    scale_width = 3 * outer_scale.shape[1] + mixer_scale.shape[1]
+    blocks = pl.pallas_call(
+        functools.partial(mixer_kernel, n),
+        out_shape=jax.ShapeDtypeStruct((n, tile, width), bf16),
+        in_specs=[
+            anywhere,
+            whole,
+            anywhere,
+            anywhere,
+            anywhere,
+            whole,
+            anywhere,
+            whole,
+            whole,
+            whole,
+            whole,
+        ],
+        out_specs=whole,
+        scratch_shapes=[
+            pltpu.VMEM((seq, depth), bf16),
+            pltpu.VMEM((seq, depth), bf16),
+            pltpu.VMEM((MATRICES, block, width), f32),
+            pltpu.VMEM((MATRICES, n * block, width), bf16),
+            pltpu.VMEM((n, 1, scale_width), f32),
+            pltpu.VMEM((seq, width), bf16),
+            pltpu.VMEM((seq, width), bf16),
+            pltpu.VMEM((seq + 8, width), f32),
+            pltpu.VMEM((seq, width), bf16),
+            pltpu.VMEM((n, 2, tile, width), f32),
+            pltpu.VMEM((n, 2, tile, width), bf16),
+            pltpu.VMEM((n, 2, tile, width), bf16),
+            pltpu.VMEM((n, tile, width), bf16),
+            pltpu.VMEM((n, tile, width), bf16),
+            dma((MATRICES + 1,)),
+            dma((MATRICES, n)),
+            dma((MATRICES, n)),
+            dma((MATRICES, n)),
+            dma((MATRICES, n)),
+            dma((MATRICES, n)),
+            dma((n,)),
+            dma((n,)),
+            dma((n,)),
+            dma((n,)),
+            dma((n,)),
+            dma((n,)),
+        ],
+        compiler_params=pltpu.CompilerParams(
+            collective_id=0, has_side_effects=True, vmem_limit_bytes=56 * 2**20
+        ),
+    )(
+        tokens,
+        mixer_gain.reshape(1, -1),
+        outer_weight,
+        inner_weight,
+        value_weight,
+        filter_taps,
+        mixer_weight,
+        outer_scale,
+        inner_scale,
+        value_scale,
+        mixer_scale,
+    )
+    return blocks.transpose(1, 0, 2).reshape(tile, n * width)
+
+
+def choose(mesh):
+    n, ntp, groups = mesh.shape["fs"], mesh.shape["tp"], mesh.shape["grp"]
+
+    def run(*args):
+        tokens, weight, mixer, scale = args[0], args[2], args[6], args[7]
+        fits = (
+            groups == 2
+            and ntp == 4
+            and n == 4
+            and weight.shape == mixer.shape
+            and weight.shape[0] % 64 == 0
+            and weight.shape[1] % 128 == 0
+            and scale.shape[1] % 128 == 0
+            and tokens.shape[0] % 256 == 0
+        )
+        return fused_device(n, *args) if fits else per_device(*args)
+
+    return run
+
+
 def solution(mesh):
     in_specs = (
         P(("grp", "fs"), None),
@@ -92,5 +547,5 @@
     )
     out_specs = P(("grp", "fs", "tp"), None)
     return jax.shard_map(
-        per_device, mesh=mesh, in_specs=in_specs, out_specs=out_specs, check_vma=False
-    )
+        choose(mesh), mesh=mesh, in_specs=in_specs, out_specs=out_specs, check_vma=False
+    )

time: 252 us -> 117 us (0.46)
  waiting for transfers between devices: 172 us -> 0 us
  Pallas kernels: 0 us -> 113 us
  blocking collectives: 34.6 us -> 0 us
  matrix products: 23.3 us -> 0 us
  between operations: 13.3 us -> 0.02 us
  other arithmetic: 8.31 us -> 0 us
  local copies, waits for them, and re-layouts: 0.05 us -> 2.9 us
    all_gather x4 -> x0, waiting for transfers between devices: 128 us -> none  [the longest x1 40.8 us: per_device(): lax.all_gather(value_weight.astype(jnp.bfloat16), 'fs', axis=0, tiled=True)]
    pallas_call x0 -> x1, Pallas kernels: none -> 113 us  [fused_device(): pl.pallas_call(functools.partial(mixer_kernel, n), out_shape=jax.ShapeDty...]
    reduce_scatter x1 -> x0, waiting for transfers between devices: 43.6 us -> none  [per_device(): lax.psum_scatter((jnp.dot(gated, mixer_full, preferred_element_type=jnp.f...]
    all_gather x4 -> x0, blocking collectives: 34.6 us -> none  [the longest x1 10.3 us: per_device(): lax.all_gather(mixer_scale, 'fs', axis=1, tiled=True)]
    dot_general x4 -> x0, matrix products: 23.3 us -> none  [the longest x3 16.7 us: add_rows(): return jnp.dot(left, piece, preferred_element_type=jnp.float32)]
    convert_element_type x4 -> x0, other arithmetic: 4.89 us -> none  [the longest x1 2.23 us: per_device(): outer_weight.astype(jnp.bfloat16)]
    reduce_sum x1 -> x0, other arithmetic: 3.1 us -> none  [normed(): inverse = lax.rsqrt(jnp.mean(values * values, axis=-1, keepdims=True) + EPS)]
  transfers between devices with their start and end apart: 5 -> 0, of which waited for: 5 -> 0; matrix products, arithmetic and copies ran while one was open for 9% -> 0% of each run, Pallas kernels for 0% -> 0%
where the time goes in v1:
time: 117 us; the launch traced here: 116 us
  Pallas kernels  113 us (97%)
  local copies, waits for them, and re-layouts  2.9 us (2%)
    pallas_call x1, Pallas kernels, fused_device(): pl.pallas_call(functools.partial(mixer_kernel, n), out_shape=jax.ShapeDty...  113 us

profile of v1, /device:TPU:1, one launch (start us, length us, event | category | flops | bytes accessed | tf_op | source)
XLA Modules:
  0.0 116.3 jit_solution(3940583968574112796)
XLA Ops:
  0.0 113.4 %shard_map.109 = bf16[4,256,512]{2,1,0:T(8,128)(2,1)} custom-call(bf16[1024,2048]{1,0:T(8,128)(2,1)} %tokens_hbm.1, f32[1,2048]{1,0:T(1,128)} %bitcast.5, f32[512,512]{1,0:T(8,128)} %w0_hbm.1, f32[512,512]{1,0:T(8,128)} %w1_hbm.1, f32[512,512]{1,0:T(8,128)} %w2_hbm.1, f32[3,512]{1,0:T(4,128)} %taps_ref.1, f32[512,512]{1,0:T(8,128)} %w3_hbm.1, ...), custom_call_target="tpu_custom_call" | custom-call | tf_op jit(solution)/shard_map/pallas_call | solution.py:450
  113.4 1.5 %copy.12 = bf16[256,4,512]{0,2,1:T(8,128)(2,1)S(1)} copy(bf16[256,4,512]{2,0,1:T(8,128)(2,1)} %bitcast.4) | data formatting | bytes 2097152 | tf_op jit(solution)/shard_map/transpose | solution.py:511
  114.9 1.4 %copy.13 = bf16[256,2048]{1,0:T(8,128)(2,1)} copy(bf16[256,2048]{0,1:T(8,128)(2,1)S(1)} %bitcast.3) | data formatting | bytes 2097152 | tf_op jit(solution)/shard_map/reshape | solution.py:511

commit v2 on v1

--- a/solution.py
+++ b/solution.py
@@ -82,6 +82,8 @@
 
 MESH = pl.DeviceIdType.MESH
 MATRICES = 4
+SPLIT = 1
+PIECES = MATRICES * SPLIT
 
 
 def mixer_kernel(
@@ -167,11 +169,17 @@
         loads[m].wait()
         held[m, pl.ds(pl.multiple_of(z * block, block), block), :] = stage[m].astype(jnp.bfloat16)
 
-    def part_of(m, b):
-        return held.at[m, pl.ds(pl.multiple_of(b * block + y * half, half), half), :]
-
-    def other_of(m, b):
-        return held.at[m, pl.ds(pl.multiple_of(b * block + (1 - y) * half, half), half), :]
+    chunk = half // SPLIT
+
+    def rows_of(p, b, side):
+        first = b * block + side * half + (p % SPLIT) * chunk
+        return held.at[p // SPLIT, pl.ds(pl.multiple_of(first, chunk), chunk), :]
+
+    def part_of(p, b):
+        return rows_of(p, b, y)
+
+    def other_of(p, b):
+        return rows_of(p, b, 1 - y)
 
     def to_left(m, b):
         return pltpu.make_async_remote_copy(
@@ -291,11 +299,22 @@
     cast(0)
     cast(1)
     pl.semaphore_wait(barrier, n - 1 + ntp - 1 + 1)
-    send_own(0)
     for d in range(1, n):
         scale_copy(d).start()
+    send_own(0)
     cast(2)
     cast(3)
+    at_end = (z == 0) | (z == n - 1)
+
+    @pl.when(at_end)
+    def _():
+        for p in range(1, PIECES):
+            send_own(p)
+
+    def send_own_inside(m):
+        @pl.when(jnp.logical_not(at_end))
+        def _():
+            send_own(m)
 
     token_load.wait()
     strip = seq // 8
@@ -304,9 +323,6 @@
     def _(i):
         at = pl.ds(pl.multiple_of(i * strip, strip), strip)
         rows[at, :] = normed(toks[at, :], gain_ref[...])
-
-    for d in range(1, n):
-        scale_arrival(d).wait_recv()
 
     product[0:8, :] = jnp.zeros((8, width), jnp.float32)
 
@@ -371,34 +387,57 @@
 
             @pl.when((b >= 0) & (b <= n - 1))
             def _():
-                from_twin(3, b).wait_recv()
+                for p in range(3 * SPLIT, PIECES):
+                    from_twin(p, b).wait_recv()
                 mix(b)
 
-    steps = [(m, s) for m in range(MATRICES) for s in range(n - 1)]
-    work = {}
-    for m, target in ((0, outer_buf), (1, inner_buf)):
-        at = (m + 1) * (n - 1)
-        work[at + 1] = [functools.partial(project_tiles, m, target, 0, 2)]
-        work[at + 2] = [functools.partial(project_tiles, m, target, 2, 4)]
-    last = 3 * (n - 1)
-    work[last + 1] = [functools.partial(gate_tile, i) for i in range(2)]
-    work[last + 2] = [functools.partial(gate_tile, i) for i in range(2, 4)]
-    for at, (m, s) in enumerate(steps):
-        relay(m, s)
-        if s == n - 2 and m < MATRICES - 1:
-            send_own(m + 1)
-        if at >= 1 and steps[at - 1][0] < 3:
-            twin_arrival(*steps[at - 1])
+    def all_twins(m):
+        for p in range(m * SPLIT, (m + 1) * SPLIT):
+            for s in range(n - 1):
+                twin_arrival(p, s)
+
+    def outer_tiles(start, stop):
+        project_tiles(0, outer_buf, start, stop)
+
+    def inner_tiles(start, stop):
+        project_tiles(1, inner_buf, start, stop)
+
+    def scales_in():
+        for d in range(1, n):
+            scale_arrival(d).wait_recv()
+
+    steps = [(p, s) for p in range(PIECES) for s in range(n - 1)]
+    per_matrix = SPLIT * (n - 1)
+    work = {
+        per_matrix + SPLIT: [
+            scales_in,
+            functools.partial(all_twins, 0),
+            functools.partial(outer_tiles, 0, 2),
+        ],
+        per_matrix + 2 * SPLIT: [functools.partial(outer_tiles, 2, 4)],
+        2 * per_matrix + SPLIT: [
+            functools.partial(all_twins, 1),
+            functools.partial(inner_tiles, 0, 2),
+        ],
+        2 * per_matrix + 2 * SPLIT: [functools.partial(inner_tiles, 2, 4)],
+        3 * per_matrix: [functools.partial(all_twins, 2)]
+        + [functools.partial(gate_tile, i) for i in range(4)]
+        + [functools.partial(mix, z)],
+    }
+    for at, (p, s) in enumerate(steps):
+        relay(p, s)
+        if s == n - 3 and p < PIECES - 1:
+            send_own_inside(p + 1)
         for task in work.get(at, ()):
             task()
-    mix(z)
-    for s in range(n - 1):
-        mix_arrived(s)
+        if p == PIECES - 1 and s >= 1:
+            mix_arrived(s - 1)
+    mix_arrived(n - 2)
 
     @pl.loop(0, n)
     def _(b):
         chip_copy(b).wait_recv()
-        out_ref[b] = (
+        out_ref[:, pl.ds(pl.multiple_of(b * width, width), width)] = (
             own_part[b, x]
             + core_in[b, x].astype(jnp.float32)
             + chip_in[b].astype(jnp.float32)
@@ -408,21 +447,21 @@
 
     for d in range(1, n):
         scale_copy(d).wait_send()
-    for m in range(MATRICES):
+    for p in range(PIECES):
 
         @pl.loop(0, n)
         def _(b):
             @pl.when((b >= z) & (z >= 1))
             def _():
-                to_left(m, b).wait_send()
+                to_left(p, b).wait_send()
 
             @pl.when((b <= z) & (z <= n - 2))
             def _():
-                to_right(m, b).wait_send()
+                to_right(p, b).wait_send()
 
             @pl.when(b != z)
             def _():
-                to_twin(m, b).wait_send()
+                to_twin(p, b).wait_send()
 
 
 def fused_device(
@@ -447,9 +486,9 @@
     bf16, f32 = jnp.bfloat16, jnp.float32
     dma = pltpu.SemaphoreType.DMA
     scale_width = 3 * outer_scale.shape[1] + mixer_scale.shape[1]
-    blocks = pl.pallas_call(
+    return pl.pallas_call(
         functools.partial(mixer_kernel, n),
-        out_shape=jax.ShapeDtypeStruct((n, tile, width), bf16),
+        out_shape=jax.ShapeDtypeStruct((tile, n * width), bf16),
         in_specs=[
             anywhere,
             whole,
@@ -480,11 +519,11 @@
             pltpu.VMEM((n, tile, width), bf16),
             pltpu.VMEM((n, tile, width), bf16),
             dma((MATRICES + 1,)),
-            dma((MATRICES, n)),
-            dma((MATRICES, n)),
-            dma((MATRICES, n)),
-            dma((MATRICES, n)),
-            dma((MATRICES, n)),
+            dma((PIECES, n)),
+            dma((PIECES, n)),
+            dma((PIECES, n)),
+            dma((PIECES, n)),
+            dma((PIECES, n)),
             dma((n,)),
             dma((n,)),
             dma((n,)),
@@ -508,7 +547,6 @@
         value_scale,
         mixer_scale,
     )
-    return blocks.transpose(1, 0, 2).reshape(tile, n * width)
 
 
 def choose(mesh):
@@ -521,7 +559,7 @@
             and ntp == 4
             and n == 4
             and weight.shape == mixer.shape
-            and weight.shape[0] % 64 == 0
+            and weight.shape[0] % (32 * SPLIT) == 0
             and weight.shape[1] % 128 == 0
             and scale.shape[1] % 128 == 0
             and tokens.shape[0] % 256 == 0

time: 117 us -> 102 us (0.87)
  Pallas kernels: 113 us -> 99.7 us
    pallas_call x1, Pallas kernels: 113 us -> 99.7 us  [fused_device(): pl.pallas_call(functools.partial(mixer_kernel, n), out_shape=jax.ShapeDty...]
    unnamed x0 -> x1, local copies, waits for them, and re-layouts: none -> 2.3 us
    transpose x1 -> x0, local copies, waits for them, and re-layouts: 1.48 us -> none  [fused_device(): return blocks.transpose(1, 0, 2).reshape(tile, n * width)]
    reshape x1 -> x0, local copies, waits for them, and re-layouts: 1.42 us -> none  [fused_device(): return blocks.transpose(1, 0, 2).reshape(tile, n * width)]
where the time goes in v2:
time: 102 us
  Pallas kernels  99.7 us (98%)
  local copies, waits for them, and re-layouts  2.3 us (2%)
    pallas_call x1, Pallas kernels, fused_device(): pl.pallas_call(functools.partial(mixer_kernel, n), out_shape=jax.ShapeDty...  99.7 us
    unnamed x1, local copies, waits for them, and re-layouts  2.3 us

profile of v2, /device:TPU:1, one launch (start us, length us, event | category | flops | bytes accessed | tf_op | source)
XLA Modules:
  0.0 102.0 jit_solution(6048983563544582661)
XLA Ops:
  0.0 99.7 %shard_map.109 = bf16[256,2048]{1,0:T(8,128)(2,1)} custom-call(bf16[1024,2048]{1,0:T(8,128)(2,1)} %tokens_hbm.1, f32[1,2048]{1,0:T(1,128)} %bitcast.1, f32[512,512]{1,0:T(8,128)} %w0_hbm.1, f32[512,512]{1,0:T(8,128)} %w1_hbm.1, f32[512,512]{1,0:T(8,128)} %w2_hbm.1, f32[3,512]{1,0:T(4,128)} %taps_ref.1, f32[512,512]{1,0:T(8,128)} %w3_hbm.1, f32[1,128]{1,0:T(1,128)} %s0_ref.1, ...), custom_call_target="tpu_custom_call" | custom-call | tf_op jit(solution)/shard_map/pallas_call | solution.py:489
  99.7 2.3 %copy.13 = bf16[256,2048]{1,0:T(8,128)(2,1)} copy(bf16[256,2048]{1,0:T(8,128)(2,1)} %shard_map.109) | data formatting | bytes 2097152
